TPU v7x, 32 devices: a whole 2x2x4 slice. The times are simulated.
32 devices in a mesh: sp: 4 (over y, x), dp: 8 (over z, core).
Axes of the slice: x: 2, y: 2, z: 4, core: 2. Of those that a mesh axis runs over, the one named last changes fastest.
Arguments:
- tokens: bfloat16 [8, 640, 2048], P('dp', 'sp'), may hold values from -42 to 42
- query_weight: bfloat16 [2048, 1024], P('dp'), may hold values from -1 to 1
- key_weight: bfloat16 [2048, 1024], P('dp'), may hold values from -1 to 1
- values: bfloat16 [8, 640, 1024], P('dp', 'sp'), may hold values from -6 to 6
- lambdas: float32 [16], replicated, may hold values from 0.3 to 0.8
- out_grad: bfloat16 [8, 640, 1024], P('dp', 'sp'), may hold values from -6 to 6
Outputs:
- tokens_grad: bfloat16 [8, 640, 2048], P('dp', 'sp')
- values_grad: bfloat16 [8, 640, 1024], P('dp', 'sp')
- query_weight_grad: float32 [2048, 1024], P('dp')
- key_weight_grad: float32 [2048, 1024], P('dp')
All inputs are finite; a program needn't handle non-finite values.
Results may differ from a plain program's by a relative error of at most 0.029.
The roundings to bfloat16 on the way count: a program that leaves them out, or rounds other values in their place, can miss the bound.
Values may be sent and summed in bfloat16 or wider, within the bound.
No kernel may reach another device: no remote copies, remote signals or barrier semaphores. Data moves between devices by JAX's collectives and lax.ppermute only.
A program may use at most 128 MiB of HBM per device.

v0:
```python
import math

import jax
import jax.numpy as jnp
from jax import lax
from jax.sharding import PartitionSpec as P

DQK = 32


NORM_EPS = 0.1
THETA = 10000.0


def rotation_tables(positions, vec_width):
    half_width = vec_width // 2
    freqs = jnp.exp(-math.log(THETA) * jnp.arange(half_width, dtype=jnp.float32) / half_width)
    angles = positions.astype(jnp.float32)[:, None] * freqs[None, :]
    return (jnp.cos(angles), jnp.sin(angles))


def rotate(field, cosine, sine_table, vec_width, sign_value):
    full_shape = field.shape
    grouped = field.reshape(full_shape[:-1] + (full_shape[-1] // vec_width, 2, vec_width // 2))
    first_half = grouped[..., 0, :]
    second_half = grouped[..., 1, :]
    cos_cols = cosine[:, None, :]
    sin_cols = sign_value * sine_table[:, None, :]
    turned = jnp.stack(
        [
            first_half * cos_cols - second_half * sin_cols,
            second_half * cos_cols + first_half * sin_cols,
        ],
        axis=-2,
    )
    return turned.reshape(full_shape)


def pair_product(pattern, first_op, second_op):
    return jnp.einsum(pattern, first_op, second_op, preferred_element_type=jnp.float32)


def head_backward(query_rot, key_rot, value_rows, grad_rows, lambda_here, cosine, sine_table):
    seq_length = query_rot.shape[0]
    head_count = lambda_here.shape[0]
    qk_width = query_rot.shape[1] // (2 * head_count)
    value_width = value_rows.shape[1] // head_count
    block_rows = math.gcd(seq_length, 512)
    block_count = seq_length // block_rows
    inv_root = 1.0 / math.sqrt(qk_width)
    query_split = query_rot.reshape(block_count, block_rows, head_count, 2, qk_width)
    key_split = key_rot.reshape(seq_length, head_count, 2, qk_width)
    value_split = value_rows.reshape(seq_length, head_count, value_width)
    grad_split = grad_rows.reshape(block_count, block_rows, head_count, value_width)
    lambda_col = lambda_here[:, None, None]
    key_positions = jnp.arange(seq_length, dtype=jnp.int32)

    def block_step(carried, inputs):
        key_sum, value_sum = carried
        query_part, grad_part, block_start = inputs
        scores = pair_product("qhmd,khmd->hmqk", query_part, key_split) * inv_root
        query_positions = block_start + jnp.arange(block_rows, dtype=jnp.int32)
        causal_mask = key_positions[None, :] <= query_positions[:, None]
        scores = jnp.where(causal_mask, scores, -jnp.inf)
        row_max = jnp.max(scores, axis=-1, keepdims=True)
        exp_scores = jnp.exp(scores - row_max)
        prob_maps = exp_scores / jnp.sum(exp_scores, axis=-1, keepdims=True)
        weights = (prob_maps[:, 0] - lambda_col * prob_maps[:, 1]).astype(jnp.bfloat16)
        mixed_out = pair_product("hqk,khe->qhe", weights, value_split)
        norm_scale = lax.rsqrt(jnp.mean(mixed_out * mixed_out, axis=-1, keepdims=True) + NORM_EPS)
        grad_float = grad_part.astype(jnp.float32)
        mixed_grad = (
            norm_scale * grad_float
            - norm_scale
            * norm_scale
            * norm_scale
            * mixed_out
            * jnp.mean(grad_float * mixed_out, axis=-1, keepdims=True)
        ).astype(jnp.bfloat16)
        weight_grad = pair_product("qhe,khe->hqk", mixed_grad, value_split)
        value_sum = value_sum + pair_product("hqk,qhe->khe", weights, mixed_grad)
        first_grad = prob_maps[:, 0] * (
            weight_grad - jnp.sum(weight_grad * prob_maps[:, 0], axis=-1, keepdims=True)
        )
        second_grad = (
            -lambda_col
            * prob_maps[:, 1]
            * (weight_grad - jnp.sum(weight_grad * prob_maps[:, 1], axis=-1, keepdims=True))
        )
        score_grad = (jnp.stack([first_grad, second_grad], axis=1) * inv_root).astype(jnp.bfloat16)
        query_grad = pair_product("hmqk,khmd->qhmd", score_grad, key_split)
        key_sum = key_sum + pair_product("hmqk,qhmd->khmd", score_grad, query_part)
        return ((key_sum, value_sum), query_grad)

    zero_init = (
        jnp.zeros((seq_length, head_count, 2, qk_width), jnp.float32),
        jnp.zeros((seq_length, head_count, value_width), jnp.float32),
    )
    block_starts = jnp.arange(block_count, dtype=jnp.int32) * block_rows
    (key_sum, value_sum), query_blocks = lax.scan(
        block_step, zero_init, (query_split, grad_split, block_starts)
    )
    query_turned = query_blocks.reshape(seq_length, head_count * 2 * qk_width)
    key_turned = key_sum.reshape(seq_length, head_count * 2 * qk_width)
    query_back = rotate(query_turned, cosine, sine_table, qk_width, -1.0).astype(jnp.bfloat16)
    key_back = rotate(key_turned, cosine, sine_table, qk_width, -1.0).astype(jnp.bfloat16)
    values_back = value_sum.reshape(seq_length, head_count * value_width).astype(jnp.bfloat16)
    return (query_back, key_back, values_back)


def body(tokens, query_weight, key_weight, values, lambdas, out_grad):
    sp_count = lax.axis_size("sp")
    dp_count = lax.axis_size("dp")
    tok_rows = tokens.shape[1]
    head_total = lambdas.shape[0]
    token_block = tokens[0]
    positions = lax.axis_index("sp") * tok_rows + jnp.arange(tok_rows, dtype=jnp.int32)
    cosine, sine_table = rotation_tables(positions, DQK)
    whole_query, whole_key = (
        lax.all_gather(query_weight, "dp", axis=0, tiled=True),
        lax.all_gather(key_weight, "dp", axis=0, tiled=True),
    )
    query_raw = jnp.dot(token_block, whole_query, preferred_element_type=jnp.float32)
    key_raw = jnp.dot(token_block, whole_key, preferred_element_type=jnp.float32)
    query_rot = rotate(query_raw, cosine, sine_table, DQK, 1.0).reshape(
        tok_rows, head_total, 2 * DQK
    )
    key_rot = rotate(key_raw, cosine, sine_table, DQK, 1.0).reshape(tok_rows, head_total, 2 * DQK)
    packed = (
        jnp.stack((query_rot, key_rot), axis=2)
        .reshape(1, tok_rows, head_total * 4 * DQK)
        .astype(jnp.bfloat16)
    )
    packed_heads, values_heads, grad_heads = (
        lax.all_to_all(packed, "sp", split_axis=2, concat_axis=1, tiled=True),
        lax.all_to_all(values, "sp", split_axis=2, concat_axis=1, tiled=True),
        lax.all_to_all(out_grad, "sp", split_axis=2, concat_axis=1, tiled=True),
    )
    heads_here = head_total // sp_count
    lambda_here = lax.dynamic_slice_in_dim(lambdas, lax.axis_index("sp") * heads_here, heads_here)
    seq_length = tok_rows * sp_count
    cosine_all, sine_all = rotation_tables(jnp.arange(seq_length, dtype=jnp.int32), DQK)
    head_split = packed_heads[0].reshape(seq_length, heads_here, 2, 2 * DQK)
    query_heads = head_split[:, :, 0].reshape(seq_length, heads_here * 2 * DQK)
    key_heads = head_split[:, :, 1].reshape(seq_length, heads_here * 2 * DQK)
    query_back, key_back, values_back = head_backward(
        query_heads, key_heads, values_heads[0], grad_heads[0], lambda_here, cosine_all, sine_all
    )
    packed_back = jnp.stack(
        (
            query_back.reshape(seq_length, heads_here, 2 * DQK),
            key_back.reshape(seq_length, heads_here, 2 * DQK),
        ),
        axis=2,
    )
    packed_back = packed_back.reshape(1, seq_length, heads_here * 4 * DQK)
    packed_tokens, values_grad = (
        lax.all_to_all(packed_back, "sp", split_axis=1, concat_axis=2, tiled=True),
        lax.all_to_all(values_back[None], "sp", split_axis=1, concat_axis=2, tiled=True),
    )
    packed_rows = packed_tokens[0]
    back_split = packed_rows.reshape(tok_rows, head_total, 2, 2 * DQK)
    query_tok = back_split[:, :, 0].reshape(tok_rows, head_total * 2 * DQK)
    key_tok = back_split[:, :, 1].reshape(tok_rows, head_total * 2 * DQK)
    contract = (((1,), (1,)), ((), ()))
    tokens_grad = lax.dot_general(
        query_tok, whole_query, contract, preferred_element_type=jnp.float32
    ) + lax.dot_general(key_tok, whole_key, contract, preferred_element_type=jnp.float32)
    outer_rows = (((0,), (0,)), ((), ()))
    grad_shard = lax.psum_scatter(
        lax.dot_general(
            token_block, packed_rows, outer_rows, preferred_element_type=jnp.float32
        ).astype(jnp.bfloat16),
        "dp",
        scatter_dimension=0,
        tiled=True,
    )
    grad_total = lax.psum(grad_shard, "sp").astype(jnp.float32)
    factor = 1.0 / math.sqrt(dp_count * seq_length)
    total_split = grad_total.reshape(grad_total.shape[0], head_total, 2, 2 * DQK)
    query_weight_grad = (
        total_split[:, :, 0].reshape(grad_total.shape[0], head_total * 2 * DQK) * factor
    )
    key_weight_grad = (
        total_split[:, :, 1].reshape(grad_total.shape[0], head_total * 2 * DQK) * factor
    )
    return (tokens_grad.astype(jnp.bfloat16)[None], values_grad, query_weight_grad, key_weight_grad)


def solution(mesh):
    in_specs = (
        P("dp", "sp", None),
        P("dp", None),
        P("dp", None),
        P("dp", "sp", None),
        P(),
        P("dp", "sp", None),
    )
    out_specs = (P("dp", "sp", None), P("dp", "sp", None), P("dp", None), P("dp", None))
    return jax.shard_map(body, mesh=mesh, in_specs=in_specs, out_specs=out_specs, check_vma=False)
```

profile of v0, /device:TPU:0, one launch (start us, length us, event | category | flops | bytes accessed | tf_op | source)
XLA Modules:
  0.0 481.4 jit_solution(5948672629820562587)
XLA Ops:
  11.9 4.1 reduce.1
  17.4 5.4 %all-to-all-start.1 = ((bf16[4,2,20480]{2,1,0:T(2,128)(2,1)}), bf16[4,2,20480]{2,1,0:T(2,128)(2,1)S(1)}, u32[]{:S(2)}, u32[]{:S(2)}) async-start(bf16[4,2,20480]{2,1,0:T(2,128)(2,1)} %reshape.233), calls=%async_computation.1 | async-start | bytes 655360 | tf_op jit(solution)/shard_map/all_to_all | solution.py:136
  23.7 4.0 reduce.2
  29.4 31.4 %all-gather.5.cloned.1.call-done = bf16[2048,1024]{0,1:T(8,128)(2,1)} async-done(((bf16[256,1024]{0,1:T(8,128)(2,1)}), bf16[2048,1024]{0,1:T(8,128)(2,1)}) %all-gather.5.cloned.1.call-update) | async-done | bytes 4194320 | tf_op jit(solution)/shard_map/all_gather | solution.py:121
  60.7 5.0 %fusion.49 = f32[160,32,2,16]{0,1,3,2:T(8,128)S(1)} fusion(bf16[32,2,16,2048]{3,2,1,0:T(8,128)(2,1)} %bitcast.235, bf16[1,160,2048]{2,1,0:T(8,128)(2,1)S(1)} %copy-done), kind=kOutput, calls=%fused_computation.61 | convolution fusion | flops 671088640 | bytes 5505024 | tf_op jit(solution)/shard_map/dot_general | solution.py:124
  65.8 43.2 %all-gather.3.cloned.1.call-done = bf16[2048,1024]{0,1:T(8,128)(2,1)} async-done(((bf16[256,1024]{0,1:T(8,128)(2,1)}), bf16[2048,1024]{0,1:T(8,128)(2,1)}) %all-gather.3.cloned.1.call-update) | async-done | bytes 4194320 | tf_op jit(solution)/shard_map/all_gather | solution.py:120
  108.9 5.0 %fusion.51 = f32[160,32,2,16]{0,1,3,2:T(8,128)S(1)} fusion(bf16[32,2,16,2048]{3,2,1,0:T(8,128)(2,1)} %bitcast.236, bf16[1,160,2048]{2,1,0:T(8,128)(2,1)S(1)} %copy-done), kind=kOutput, calls=%fused_computation.63 | convolution fusion | flops 671088640 | bytes 5505024 | tf_op jit(solution)/shard_map/dot_general | solution.py:123
  115.0 3.9 all-to-all-start.2
  121.0 11.7 %copy.159 = bf16[1,160,2048]{1,0,2:T(2,128)(2,1)S(1)} copy(bf16[1,160,2048]{1,2,0:T(8,128)(2,1)S(1)} %bitcast.234) | data formatting | bytes 1310720 | tf_op jit(solution)/shard_map/convert_element_type | solution.py:132
  132.8 12.6 %reduce = bf16[2048,160]{1,0:T(8,128)(2,1)} reduce(bf16[2048,1,160]{2,1,0:T(2,128)(2,1)S(1)} %bitcast.228, bf16[]{:T(256)} %broadcast.188), dimensions={1}, to_apply=%bitcast.164.reduce_sub_computation | reduce | bytes 1310722
  145.3 3.4 reshape.231
  149.5 4.2 all-to-all-start
  169.3 130.5 %while.16 = (s32[]{:T(128)}, f32[640,4,2,32]{0,3,2,1:T(8,128)}, f32[640,4,64]{0,2,1:T(8,128)}, f32[5,128,4,2,32]{1,0,4,3,2:T(8,128)}, bf16[5,128,4,2,32]{1,4,3,2...) while((s32[]{:T(128)}, f32[640,4,2,32]{0,3,2,1:T(8,128)}, ...), condition=%wide.region_7.8_spmd.clone, body=%wide.region_0.7_spmd.clone.sunk | while | flops 389075456 | bytes 51640196 | solution.py:100
  170.8 3.4 fusion.143
  183.1 2.7 fusion.145
  189.9 4.7 dynamic_update_slice.7
  196.0 3.4 fusion.143
  216.2 4.7 dynamic_update_slice.7
  222.3 3.4 fusion.143
  235.7 2.7 fusion.145
  242.6 4.7 dynamic_update_slice.7
  248.7 3.4 fusion.143
  268.9 4.7 dynamic_update_slice.7
  275.0 3.4 fusion.143
  295.2 4.7 dynamic_update_slice.7
  303.8 4.6 reduce.3
  308.9 11.9 %all_to_all.78 = bf16[4,2,40960]{2,1,0:T(2,128)(2,1)S(1)} all-to-all(bf16[4,2,40960]{2,1,0:T(2,128)(2,1)S(1)} %reshape.237), channel_id=1, replica_groups=mesh['sp'=4,'dp'=8] {'sp'}, dimensions={0} | all-to-all | bytes 1310720 | tf_op jit(solution)/shard_map/all_to_all | solution.py:158
  322.3 5.6 %convert_bitcast_fusion = bf16[2048,2048]{0,1:T(8,128)(2,1)} fusion(bf16[160,2048]{1,0:T(8,128)(2,1)S(1)} %bitcast.244, bf16[1,160,2048]{2,1,0:T(8,128)(2,1)S(1)} %copy-done), kind=kOutput, calls=%fused_computation.60 | convolution fusion | flops 1346371584 | bytes 9699328 | tf_op jit(solution)/shard_map/dot_general | solution.py:171
  333.3 3.5 all-to-all-start.4
  336.8 79.1 %reduce-scatter.2.cloned.1.call-done = bf16[256,2048]{0,1:T(8,128)(2,1)} async-done(((bf16[2048,2048]{0,1:T(8,128)(2,1)}), bf16[256,2048]{0,1:T(8,128)(2,1)}) %reduce-scatter.2.cloned.1.call-update) | async-done | bytes 1048592 | tf_op jit(solution)/shard_map/reduce_scatter | solution.py:170
  420.2 3.2 fusion.64
  425.7 44.7 %all-reduce.2.cloned.1.call-done = bf16[256,16,2,64]{0,3,1,2:T(8,128)(2,1)} async-done(((bf16[256,16,2,64]{0,3,1,2:T(8,128)(2,1)}), bf16[256,16,2,64]{0,3,1,2:T(8,128)(2,1)}) %all-reduce.2.cloned.1.call-update) | async-done | bytes 1048592 | tf_op jit(solution)/shard_map/psum | solution.py:178
  (235 shorter events, 134.3 us)
Async XLA Ops:
  7.2 53.6 %copy-start = (bf16[1,160,2048]{2,1,0:T(8,128)(2,1)S(1)}, bf16[1,160,2048]{2,1,0:T(8,128)(2,1)}, u32[]{:S(2)}) copy-start(bf16[1,160,2048]{2,1,0:T(8,128)(2,1)} %param.8) | copy-start | bytes 1966084
  7.2 53.5 %all-gather.5.cloned.1.call-start = ((), (), s32[]{:S(2)}) async-start(), calls=%async_computation.7 | async-start | bytes 4718592 | tf_op jit(solution)/shard_map/all_gather | solution.py:121
  9.4 99.5 %all-gather.3.cloned.1.call-start = ((), (), s32[]{:S(2)}) async-start(), calls=%async_computation.6 | async-start | bytes 4718592 | tf_op jit(solution)/shard_map/all_gather | solution.py:120
  11.9 11.0 %copy-start.16 = (bf16[1,160,1024]{2,1,0:T(8,128)(2,1)S(1)}, bf16[1,160,1024]{2,1,0:T(8,128)(2,1)}, u32[]{:S(2)}) copy-start(bf16[1,160,1024]{2,1,0:T(8,128)(2,1)} %param.13) | copy-start | bytes 983044
  17.4 97.6 %all-to-all-start.1 = ((bf16[4,2,20480]{2,1,0:T(2,128)(2,1)}), bf16[4,2,20480]{2,1,0:T(2,128)(2,1)S(1)}, u32[]{:S(2)}, u32[]{:S(2)}) async-start(bf16[4,2,20480]{2,1,0:T(2,128)(2,1)} %reshape.233), calls=%async_computation.1 | async-start | bytes 655360 | tf_op jit(solution)/shard_map/all_to_all | solution.py:136
  115.0 5.0 %copy-start.8 = (bf16[4,2,20480]{2,1,0:T(2,128)(2,1)}, bf16[4,2,20480]{2,1,0:T(2,128)(2,1)S(1)}, u32[]{:S(2)}) copy-start(bf16[4,2,20480]{2,1,0:T(2,128)(2,1)S(1)} %all-to-all-done.1) | copy-start | bytes 983044
  115.0 33.7 %all-to-all-start.2 = ((bf16[4,2,20480]{2,1,0:T(2,128)(2,1)}), bf16[4,2,20480]{2,1,0:T(2,128)(2,1)S(1)}, u32[]{:S(2)}, u32[]{:S(2)}) async-start(bf16[4,2,20480]{2,1,0:T(2,128)(2,1)} %reshape.235), calls=%async_computation.2 | async-start | bytes 655360 | tf_op jit(solution)/shard_map/all_to_all | solution.py:137
  145.3 8.4 %copy-start.17 = (f32[16]{0:T(128)S(1)}, f32[16]{0:T(128)}, u32[]{:S(2)}) copy-start(f32[16]{0:T(128)} %param.12) | copy-start | bytes 196
  145.3 8.7 %copy-start.9 = (bf16[4,2,20480]{2,1,0:T(2,128)(2,1)S(1)}, bf16[4,2,20480]{2,1,0:T(2,128)(2,1)}, u32[]{:S(2)}) copy-start(bf16[4,2,20480]{2,1,0:T(2,128)(2,1)} %copy-done.8) | copy-start | bytes 983044
  149.5 13.5 %all-to-all-start = ((bf16[4,2,40960]{2,1,0:T(2,128)(2,1)}), bf16[4,2,40960]{2,1,0:T(2,128)(2,1)S(1)}, u32[]{:S(2)}, u32[]{:S(2)}) async-start(bf16[4,2,40960]{2,1,0:T(2,128)(2,1)} %reshape.231), calls=%async_computation | async-start | bytes 1310720 | tf_op jit(solution)/shard_map/all_to_all | solution.py:135
  153.7 262.3 %reduce-scatter.2.cloned.1.call-start = ((), (), s32[]{:S(2)}) async-start(), calls=%async_computation.8 | async-start | bytes 9437184 | tf_op jit(solution)/shard_map/reduce_scatter | solution.py:170
  169.3 4.9 %copy-start.13 = (bf16[640,4,2,32]{0,3,2,1:T(8,128)(2,1)}, bf16[640,4,2,32]{0,3,2,1:T(8,128)(2,1)S(1)}, u32[]{:S(2)}) copy-start(bf16[640,4,2,32]{0,3,2,1:T(8,128)(2,1)S(1)} %get-tuple-element.384) | copy-start | bytes 983044 | tf_op jit(solution)/shard_map/while
  185.8 2.8 copy-start.4
  188.6 6.0 %copy-start.14 = (bf16[640,4,2,32]{0,3,2,1:T(8,128)(2,1)S(1)}, bf16[640,4,2,32]{0,3,2,1:T(8,128)(2,1)}, u32[]{:S(2)}) copy-start(bf16[640,4,2,32]{0,3,2,1:T(8,128)(2,1)} %copy-done.13) | copy-start | bytes 983044 | tf_op jit(solution)/shard_map/while
  189.9 4.7 copy-start.5
  194.6 4.9 %copy-start.13 = (bf16[640,4,2,32]{0,3,2,1:T(8,128)(2,1)}, bf16[640,4,2,32]{0,3,2,1:T(8,128)(2,1)S(1)}, u32[]{:S(2)}) copy-start(bf16[640,4,2,32]{0,3,2,1:T(8,128)(2,1)S(1)} %get-tuple-element.384) | copy-start | bytes 983044 | tf_op jit(solution)/shard_map/while
  212.2 2.8 copy-start.4
  214.9 6.0 %copy-start.14 = (bf16[640,4,2,32]{0,3,2,1:T(8,128)(2,1)S(1)}, bf16[640,4,2,32]{0,3,2,1:T(8,128)(2,1)}, u32[]{:S(2)}) copy-start(bf16[640,4,2,32]{0,3,2,1:T(8,128)(2,1)} %copy-done.13) | copy-start | bytes 983044 | tf_op jit(solution)/shard_map/while
  216.2 4.7 copy-start.5
  220.9 4.9 %copy-start.13 = (bf16[640,4,2,32]{0,3,2,1:T(8,128)(2,1)}, bf16[640,4,2,32]{0,3,2,1:T(8,128)(2,1)S(1)}, u32[]{:S(2)}) copy-start(bf16[640,4,2,32]{0,3,2,1:T(8,128)(2,1)S(1)} %get-tuple-element.384) | copy-start | bytes 983044 | tf_op jit(solution)/shard_map/while
  238.5 2.8 copy-start.4
  241.2 6.0 %copy-start.14 = (bf16[640,4,2,32]{0,3,2,1:T(8,128)(2,1)S(1)}, bf16[640,4,2,32]{0,3,2,1:T(8,128)(2,1)}, u32[]{:S(2)}) copy-start(bf16[640,4,2,32]{0,3,2,1:T(8,128)(2,1)} %copy-done.13) | copy-start | bytes 983044 | tf_op jit(solution)/shard_map/while
  242.6 4.7 copy-start.5
  247.2 4.9 %copy-start.13 = (bf16[640,4,2,32]{0,3,2,1:T(8,128)(2,1)}, bf16[640,4,2,32]{0,3,2,1:T(8,128)(2,1)S(1)}, u32[]{:S(2)}) copy-start(bf16[640,4,2,32]{0,3,2,1:T(8,128)(2,1)S(1)} %get-tuple-element.384) | copy-start | bytes 983044 | tf_op jit(solution)/shard_map/while
  267.6 6.0 %copy-start.14 = (bf16[640,4,2,32]{0,3,2,1:T(8,128)(2,1)S(1)}, bf16[640,4,2,32]{0,3,2,1:T(8,128)(2,1)}, u32[]{:S(2)}) copy-start(bf16[640,4,2,32]{0,3,2,1:T(8,128)(2,1)} %copy-done.13) | copy-start | bytes 983044 | tf_op jit(solution)/shard_map/while
  268.9 4.7 copy-start.5
  273.6 4.9 %copy-start.13 = (bf16[640,4,2,32]{0,3,2,1:T(8,128)(2,1)}, bf16[640,4,2,32]{0,3,2,1:T(8,128)(2,1)S(1)}, u32[]{:S(2)}) copy-start(bf16[640,4,2,32]{0,3,2,1:T(8,128)(2,1)S(1)} %get-tuple-element.384) | copy-start | bytes 983044 | tf_op jit(solution)/shard_map/while
  293.9 6.0 %copy-start.14 = (bf16[640,4,2,32]{0,3,2,1:T(8,128)(2,1)S(1)}, bf16[640,4,2,32]{0,3,2,1:T(8,128)(2,1)}, u32[]{:S(2)}) copy-start(bf16[640,4,2,32]{0,3,2,1:T(8,128)(2,1)} %copy-done.13) | copy-start | bytes 983044 | tf_op jit(solution)/shard_map/while
  295.2 4.7 copy-start.5
  333.3 84.9 %all-to-all-start.4 = ((bf16[4,2,20480]{2,1,0:T(2,128)(2,1)}), bf16[4,2,20480]{2,1,0:T(2,128)(2,1)S(1)}, u32[]{:S(2)}, u32[]{:S(2)}) async-start(bf16[4,2,20480]{2,1,0:T(2,128)(2,1)} %reshape.239), calls=%async_computation.4 | async-start | bytes 655360 | tf_op jit(solution)/shard_map/all_to_all | solution.py:159
  336.8 133.6 %all-reduce.2.cloned.1.call-start = ((), (), s32[]{:S(2)}) async-start(), calls=%async_computation.9 | async-start | bytes 2097152 | tf_op jit(solution)/shard_map/psum | solution.py:178
  420.2 3.8 copy-start.7
  (22 other events, 43.1 us)
Sparse Core Ops, SparseCore 0:
  10.2 50.5 all-gather.4
  62.9 46.0 all-gather.2
  328.0 87.8 reduce-scatter.1
  419.4 50.9 all-reduce.1
where the time goes:
time: 488 us; the launch traced here: 481 us
  waiting for transfers between devices  200 us (41%)
  matrix products  99.6 us (20%)
  local copies, waits for them, and re-layouts  84.4 us (17%)
  other arithmetic  53 us (11%)
  starting transfers between devices  17 us (3%)
  between operations  14.5 us (3%)
  blocking collectives  11.9 us (2%)
    reduce_scatter x1, waiting for transfers between devices, body(): lax.psum_scatter(lax.dot_general(token_block, packed_rows, outer_rows, pr...  79.1 us
    psum x1, waiting for transfers between devices, body(): grad_total = lax.psum(grad_shard, 'sp').astype(jnp.float32)  44.7 us
    all_gather x1, waiting for transfers between devices, body(): lax.all_gather(query_weight, 'dp', axis=0, tiled=True)  43.2 us
    dot_general x20, matrix products, pair_product(): jnp.einsum(pattern, first_op, second_op, preferred_element_type=jnp.float32)  34.7 us
    all_gather x1, waiting for transfers between devices, body(): lax.all_gather(key_weight, 'dp', axis=0, tiled=True)  31.4 us
    unnamed x7, other arithmetic  27.8 us
    unnamed x44, local copies, waits for them, and re-layouts  24 us
    dynamic_update_slice x5, local copies, waits for them, and re-layouts, head_backward(): lax.scan(block_step, zero_init, (query_split, grad_split, block_starts))  23.3 us
  transfers between devices with their start and end apart: 8, of which 5 were waited for; matrix products, arithmetic and copies ran while one was open for 16% of the time, Pallas kernels for 0%

commit v1 on v0

--- a/solution.py
+++ b/solution.py
@@ -1,8 +1,11 @@
+import functools
 import math
 
 import jax
 import jax.numpy as jnp
 from jax import lax
+from jax.experimental import pallas as pl
+from jax.experimental.pallas import tpu as pltpu
 from jax.sharding import PartitionSpec as P
 
 DQK = 32
@@ -108,7 +111,7 @@
     return (query_back, key_back, values_back)
 
 
-def body(tokens, query_weight, key_weight, values, lambdas, out_grad):
+def general_body(tokens, query_weight, key_weight, values, lambdas, out_grad):
     sp_count = lax.axis_size("sp")
     dp_count = lax.axis_size("dp")
     tok_rows = tokens.shape[1]
@@ -187,6 +190,432 @@
     return (tokens_grad.astype(jnp.bfloat16)[None], values_grad, query_weight_grad, key_weight_grad)
 
 
+LANES = 128
+BF16 = jnp.bfloat16
+F32 = jnp.float32
+MIB = 1 << 20
+
+
+def dot(a, b, dims=(((1,), (0,)), ((), ()))):
+    return lax.dot_general(a, b, dims, preferred_element_type=F32)
+
+
+def call(kernel, name, outs, scratch, in_specs, flops, limit, *args):
+    moved = sum(math.prod(a.shape) * a.dtype.itemsize for a in (*args, *outs))
+    vmem = pl.BlockSpec(memory_space=pltpu.VMEM)
+    smem = pl.BlockSpec(memory_space=pltpu.SMEM)
+    return pl.pallas_call(
+        kernel,
+        name=name,
+        out_shape=outs,
+        in_specs=[smem if k == "s" else vmem for k in in_specs],
+        out_specs=[vmem] * len(outs),
+        scratch_shapes=scratch,
+        compiler_params=pltpu.CompilerParams(vmem_limit_bytes=limit * MIB),
+        cost_estimate=pl.CostEstimate(flops=flops, bytes_accessed=moved, transcendentals=0),
+    )(*args)
+
+
+def shape(dims, dtype):
+    return jax.ShapeDtypeStruct(dims, dtype)
+
+
+def aligned(value, step):
+    return pl.multiple_of(value, step)
+
+
+def turn(tile, cosine, sine, sign):
+    half = cosine.shape[0]
+    parts = []
+    for start in range(0, tile.shape[0], 2 * half):
+        a = tile[start : start + half]
+        b = tile[start + half : start + 2 * half]
+        parts.append(a * cosine - b * (sign * sine))
+        parts.append(b * cosine + a * (sign * sine))
+    return jnp.concatenate(parts, axis=0)
+
+
+def pack_kernel(heads, width, index, wq, wk, values, grads, w_out, *vg_outs):
+    me = index[0]
+    cols = heads * 2 * width
+    vcols = vg_outs[0].shape[1] // 2
+    mine = pl.ds(aligned(me * cols, LANES), cols)
+    w_out[:, :cols] = wq[:, mine]
+    w_out[:, cols:] = wk[:, mine]
+    for k, out in enumerate(vg_outs):
+        theirs = pl.ds(aligned((me ^ k) * vcols, LANES), vcols)
+        out[:, :vcols] = values[:, theirs]
+        out[:, vcols:] = grads[:, theirs]
+
+
+def attention_kernel(
+    heads, width, index, lambdas, cosine, sine,
+    t_own, t_x, t_y, t_da, t_db,
+    w0, w1, w2, w3, o0, o1, o2, o3,
+    g0, g1, g2, g3,
+    tok, wfull, back_t, back, vgrad,
+    raw, rot_t, k_nat, v_nat, v_t, g_t, e_ref, mg_ref, sgm, acc,
+):
+    me, core, zed = index[0], index[1], index[2]
+    rows = t_own.shape[0]
+    half = rows // 2
+    seq = tok.shape[0]
+    cols = heads * 2 * width
+    vcols = v_nat.shape[1]
+    ve = vcols // heads
+    blocks = seq // LANES
+    wrows = w0.shape[0]
+    inv_root = 1.0 / math.sqrt(width)
+    for k, piece in ((0, t_own), (1, t_x), (2, t_y)):
+        tok[pl.ds(aligned((me ^ k) * rows, half), rows), :] = piece[...]
+    tok[pl.ds(aligned((me ^ 3) * rows, half), half), :] = t_da[...]
+    tok[pl.ds(aligned((me ^ 3) * rows + half, half), half), :] = t_db[...]
+    for k, (own, other) in enumerate(((w0, o0), (w1, o1), (w2, o2), (w3, o3))):
+        base = (zed ^ k) * 2
+        wfull[pl.ds(aligned((base + core) * wrows, wrows), wrows), :] = own[...]
+        wfull[pl.ds(aligned((base + 1 - core) * wrows, wrows), wrows), :] = other[...]
+    for n in range(0, 2 * cols, 256):
+        raw[:, n : n + 256] = dot(tok[...], wfull[:, n : n + 256])
+    for b in range(blocks):
+        at = slice(b * LANES, (b + 1) * LANES)
+        cos_b, sin_b = cosine[:, at], sine[:, at]
+        for r in range(0, 2 * cols, LANES):
+            turned = turn(jnp.transpose(raw[at, r : r + LANES]), cos_b, sin_b, 1.0)
+            rot_t[r : r + LANES, at] = turned.astype(BF16)
+            if r >= cols:
+                k_nat[at, r - cols : r - cols + LANES] = jnp.transpose(turned).astype(BF16)
+    stage = raw
+    for k, piece in enumerate((g0, g1, g2, g3)):
+        stage[pl.ds(aligned((me ^ k) * rows, half), rows), :] = piece[...].astype(F32)
+    v_nat[...] = stage[:, :vcols].astype(BF16)
+    for b in range(blocks):
+        at = slice(b * LANES, (b + 1) * LANES)
+        for r in range(0, vcols, LANES):
+            v_t[r : r + LANES, at] = jnp.transpose(stage[at, r : r + LANES]).astype(BF16)
+            g_t[r : r + LANES, at] = jnp.transpose(stage[at, vcols + r : vcols + r + LANES])
+
+    scale2 = inv_root * math.log2(math.e)
+    row_id = lax.broadcasted_iota(jnp.int32, (LANES, 2 * LANES), 0)
+    col_id = lax.broadcasted_iota(jnp.int32, (LANES, 2 * LANES), 1)
+    keep = row_id <= jnp.where(col_id < LANES, col_id, col_id - LANES)
+    lane = lax.broadcasted_iota(jnp.int32, (LANES, LANES), 1)
+    for h in range(heads):
+        pair = (h // 2) * LANES
+        odd = h % 2
+        lam = lambdas[me * heads + h]
+        zero = jnp.zeros((width, LANES), BF16)
+        for i in reversed(range(blocks)):
+            at = slice(i * LANES, (i + 1) * LANES)
+            upto = (i + 1) * LANES
+            q_t = rot_t[h * 2 * width : (h + 1) * 2 * width, at]
+            diag = [
+                jnp.concatenate([q_t[:width], zero], axis=1),
+                jnp.concatenate([zero, q_t[width:]], axis=1),
+            ]
+            blank = jnp.zeros((2 * width, 2 * LANES), BF16)
+            q_rhs = jnp.concatenate([blank, *diag] if odd else [*diag, blank], axis=0)
+            top = jnp.full((8, 2 * LANES), -1e30, F32)
+            for j in range(i + 1):
+                ub = slice(j * LANES, (j + 1) * LANES)
+                s = dot(k_nat[ub, pair : pair + LANES], q_rhs)
+                if j == i:
+                    s = jnp.where(keep, s, -1e30)
+                e_ref[ub, :] = s
+                top = jnp.maximum(top, jnp.max(s.reshape(LANES // 8, 8, 2 * LANES), axis=0))
+            top = jnp.max(top, axis=0, keepdims=True) * scale2
+            total = jnp.zeros((8, 2 * LANES), F32)
+            for j in range(i + 1):
+                ub = slice(j * LANES, (j + 1) * LANES)
+                e = jnp.exp2(e_ref[ub, :] * scale2 - top)
+                e_ref[ub, :] = e
+                total = total + jnp.sum(e.reshape(LANES // 8, 8, 2 * LANES), axis=0)
+            inv = 1.0 / jnp.sum(total, axis=0, keepdims=True)
+            r1, r2 = inv[:, :LANES], inv[:, LANES:]
+            a2 = lam * r2
+            for j in range(i + 1):
+                ub = slice(j * LANES, (j + 1) * LANES)
+                mix = e_ref[ub, :LANES] * r1 - e_ref[ub, LANES:] * a2
+                sgm[ub, 2 * LANES :] = mix.astype(BF16)
+            ho = dot(v_t[h * ve : (h + 1) * ve, :upto], sgm[:upto, 2 * LANES :])
+            g = g_t[h * ve : (h + 1) * ve, at]
+            norm = lax.rsqrt(jnp.mean(ho * ho, axis=0, keepdims=True) + NORM_EPS)
+            along = jnp.mean(g * ho, axis=0, keepdims=True)
+            ob = (norm * g - norm * norm * norm * ho * along).astype(BF16)
+            ob_blank = jnp.zeros_like(ob)
+            ob_rhs = jnp.concatenate([ob_blank, ob] if odd else [ob, ob_blank], axis=0)
+            d1 = jnp.zeros((8, LANES), F32)
+            d2 = jnp.zeros((8, LANES), F32)
+            for j in range(i + 1):
+                ub = slice(j * LANES, (j + 1) * LANES)
+                mg = dot(v_nat[ub, pair : pair + LANES], ob_rhs)
+                mg_ref[ub, :] = mg
+                d1 = d1 + jnp.sum((e_ref[ub, :LANES] * mg).reshape(LANES // 8, 8, LANES), axis=0)
+                d2 = d2 + jnp.sum((e_ref[ub, LANES:] * mg).reshape(LANES // 8, 8, LANES), axis=0)
+            d1 = jnp.sum(d1, axis=0, keepdims=True) * r1
+            d2 = jnp.sum(d2, axis=0, keepdims=True) * r2
+            f1 = r1 * inv_root
+            f2 = a2 * (-inv_root)
+            for j in range(i + 1):
+                ub = slice(j * LANES, (j + 1) * LANES)
+                mg = mg_ref[ub, :]
+                sgm[ub, :LANES] = (e_ref[ub, :LANES] * f1 * (mg - d1)).astype(BF16)
+                sgm[ub, LANES : 2 * LANES] = (e_ref[ub, LANES:] * f2 * (mg - d2)).astype(BF16)
+            k_t = rot_t[cols + h * 2 * width : cols + (h + 1) * 2 * width, :upto]
+            qt = dot(k_t, sgm[:upto, : 2 * LANES])
+            qt = jnp.concatenate([qt[:width, :LANES], qt[width:, LANES:]], axis=0)
+            qt = turn(qt, cosine[:, at], sine[:, at], -1.0)
+            back_t[h * 2 * width : (h + 1) * 2 * width, at] = qt.astype(BF16)
+            both = [q_t.astype(F32), ob.astype(F32)]
+            nat = jnp.transpose(jnp.concatenate(both if odd else both[::-1], axis=0))
+            k_at = 0 if odd else ve
+            v_at = 2 * width if odd else 0
+            rhs = jnp.concatenate(
+                [
+                    jnp.where((lane >= start) & (lane < start + size), nat, 0.0)
+                    for start, size in ((k_at, width), (k_at + width, width), (v_at, ve))
+                ],
+                axis=0,
+            ).astype(BF16)
+            term = dot(sgm[:upto, :], rhs)
+            if i == blocks - 1:
+                acc[odd, :, :] = term
+            else:
+                acc[odd, :upto, :] += term
+        k_at = 0 if odd else ve
+        for b in range(blocks):
+            at = slice(b * LANES, (b + 1) * LANES)
+            kt = jnp.transpose(acc[odd, at, :])[k_at : k_at + 2 * width]
+            kt = turn(kt, cosine[:, at], sine[:, at], -1.0)
+            back_t[cols + h * 2 * width : cols + (h + 1) * 2 * width, at] = kt.astype(BF16)
+            if odd:
+                tile = jnp.where(lane < ve, acc[0, at, :], acc[1, at, :])
+                vgrad[at, pair : pair + LANES] = tile.astype(BF16)
+    for b in range(blocks):
+        at = slice(b * LANES, (b + 1) * LANES)
+        for r in range(0, 2 * cols, LANES):
+            tile = back_t[r : r + LANES, at].astype(F32)
+            back[at, r : r + LANES] = jnp.transpose(tile).astype(BF16)
+
+
+def weight_grad_kernel(index, back_t, tok, keep, send):
+    core = index[1]
+    step = keep.shape[2]
+    for z in range(keep.shape[0]):
+        for part, out in ((core, keep), (1 - core, send)):
+            at = pl.ds(aligned((2 * z + part) * step, LANES), step)
+            out[z] = dot(back_t[...], tok[:, at]).astype(BF16)
+
+
+def token_grad_kernel(index, back, wfull, send_x, send_y, keep_x, keep_y, own, order):
+    me = index[0]
+    seq = back.shape[0]
+    rows = seq // 4
+    half = rows // 2
+    places = ((1, 0), (3, 0), (2, 1), (3, 1), (2, 0), (1, 1), (0, 0), (0, 1))
+    for n, (k, part) in enumerate(places):
+        at = pl.ds(aligned((me ^ k) * rows + part * half, half), half)
+        order[n * half : (n + 1) * half, :] = back[at, :]
+    for n in range(0, wfull.shape[0], 256):
+        at = slice(n, n + 256)
+        part = dot(order[...], wfull[at, :], (((1,), (1,)), ((), ())))
+        send_x[:, at] = part[: 2 * half].astype(BF16)
+        send_y[:, at] = part[2 * half : 4 * half].astype(BF16)
+        keep_y[:, at] = part[4 * half : 5 * half]
+        keep_x[:, at] = part[5 * half : 6 * half]
+        own[:, at] = part[6 * half :]
+
+
+def pair_sum_kernel(index, keep, got, own, s1, s2, s3):
+    zed = index[2]
+    for k, out in enumerate((own, s1, s2, s3)):
+        at = zed ^ k
+        out[...] = (keep[at].astype(F32) + got[at].astype(F32)).astype(out.dtype)
+
+
+def depth_sum_kernel(own, r1, r2, r3, out):
+    total = own[...] + r1[...].astype(F32) + r2[...].astype(F32) + r3[...].astype(F32)
+    out[...] = jnp.transpose(total).astype(BF16)
+
+
+def place_kernel(factor, cols, index, own, got_x, got_y, da, db, wq, wk):
+    me = index[0]
+    half = da.shape[0]
+    everything = slice(None)
+    for k, piece, at in (
+        (0, own, everything),
+        (1, got_x, everything),
+        (2, got_y, everything),
+        (3, da, slice(0, half)),
+        (3, db, slice(half, 2 * half)),
+    ):
+        theirs = pl.ds(aligned((me ^ k) * cols, LANES), cols)
+        wq[at, theirs] = piece[:, :cols].astype(F32) * factor
+        wk[at, theirs] = piece[:, cols:].astype(F32) * factor
+
+
+def values_kernel(index, vgrad, r1, r2, r3, out):
+    me = index[0]
+    rows = r1.shape[0]
+    cols = r1.shape[1]
+    mine = pl.ds(aligned(me * rows, rows // 2), rows)
+    out[:, pl.ds(aligned(me * cols, LANES), cols)] = vgrad[mine, :]
+    for k, piece in ((1, r1), (2, r2), (3, r3)):
+        out[:, pl.ds(aligned((me ^ k) * cols, LANES), cols)] = piece[...]
+
+
+def flip(value, axis, mask):
+    count = lax.axis_size(axis)
+    return lax.ppermute(value, axis, [(i, i ^ mask) for i in range(count)])
+
+
+def quarter_body(tokens, query_weight, key_weight, values, lambdas, out_grad):
+    sp_count = lax.axis_size("sp")
+    dp_count = lax.axis_size("dp")
+    rows, depth = tokens.shape[1:]
+    head_total = lambdas.shape[0]
+    heads = head_total // sp_count
+    seq = rows * sp_count
+    cols = heads * 2 * DQK
+    vcols = values.shape[2] // sp_count
+    wrows = query_weight.shape[0]
+    half = rows // 2
+    me = lax.axis_index("sp")
+    line = lax.axis_index("dp")
+    index = jnp.stack([me, line % 2, line // 2]).astype(jnp.int32)
+    cosine, sine = rotation_tables(jnp.arange(seq, dtype=jnp.int32), DQK)
+    own_tok = tokens[0]
+    tok_x = flip(own_tok, "sp", 1)
+    tok_y = flip(own_tok, "sp", 2)
+    w_own, *vg = call(
+        functools.partial(pack_kernel, heads, DQK),
+        "pack",
+        [shape((wrows, 2 * cols), BF16)] + [shape((rows, 2 * vcols), BF16)] * 4,
+        [],
+        "svvvv",
+        1 << 20,
+        16,
+        index, query_weight, key_weight, values[0], out_grad[0],
+    )
+    w_line = [w_own] + [flip(w_own, "dp", 2 * k) for k in (1, 2, 3)]
+    vg = [vg[0]] + [flip(vg[k], "sp", k) for k in (1, 2, 3)]
+    w_other = [flip(w, "dp", 1) for w in w_line]
+    tok_da = flip(tok_x[:half], "sp", 2)
+    tok_db = flip(tok_y[half:], "sp", 1)
+    pair_cols = heads * DQK * 2
+    tok, wfull, back_t, back, vgrad = call(
+        functools.partial(attention_kernel, heads, DQK),
+        "attention",
+        [
+            shape((seq, depth), BF16),
+            shape((depth, 2 * cols), BF16),
+            shape((2 * cols, seq), BF16),
+            shape((seq, 2 * cols), BF16),
+            shape((seq, vcols), BF16),
+        ],
+        [
+            pltpu.VMEM((seq, 2 * max(cols, vcols)), F32),
+            pltpu.VMEM((2 * cols, seq), BF16),
+            pltpu.VMEM((seq, pair_cols), BF16),
+            pltpu.VMEM((seq, vcols), BF16),
+            pltpu.VMEM((vcols, seq), BF16),
+            pltpu.VMEM((vcols, seq), F32),
+            pltpu.VMEM((seq, 2 * LANES), F32),
+            pltpu.VMEM((seq, LANES), F32),
+            pltpu.VMEM((seq, 3 * LANES), BF16),
+            pltpu.VMEM((2, seq, LANES), F32),
+        ],
+        "ss" + "v" * 19,
+        10 * seq * depth * cols,
+        40,
+        index, lambdas, cosine.T, sine.T,
+        own_tok, tok_x, tok_y, tok_da, tok_db,
+        *w_line, *w_other, *vg,
+    )
+    chips = dp_count // 2
+    keep_w, send_w = call(
+        weight_grad_kernel,
+        "weight_grad",
+        [shape((chips, 2 * cols, wrows), BF16)] * 2,
+        [],
+        "svv",
+        4 * seq * depth * cols,
+        24,
+        index, back_t, tok,
+    )
+    got_w = flip(send_w, "dp", 1)
+    send_x, send_y, keep_x, keep_y, own_t = call(
+        token_grad_kernel,
+        "token_grad",
+        [shape((rows, depth), BF16)] * 2
+        + [shape((half, depth), F32)] * 2
+        + [shape((rows, depth), F32)],
+        [pltpu.VMEM((seq, 2 * cols), BF16)],
+        "svv",
+        4 * seq * depth * cols,
+        24,
+        index, back, wfull,
+    )
+    got_x = flip(send_x, "sp", 1)
+    got_y = flip(send_y, "sp", 2)
+    own_w, *sums = call(
+        pair_sum_kernel,
+        "pair_sum",
+        [shape((2 * cols, wrows), F32)] + [shape((2 * cols, wrows), BF16)] * 3,
+        [],
+        "svv",
+        1 << 20,
+        16,
+        index, keep_w, got_w,
+    )
+    got_line = [flip(w, "dp", 2 * k) for k, w in zip((1, 2, 3), sums)]
+    v_out = [
+        flip(lax.dynamic_slice_in_dim(vgrad, (me ^ k) * rows, rows, 0), "sp", k) for k in (1, 2, 3)
+    ]
+    pass_y = (keep_y + got_x[half:].astype(F32)).astype(BF16)
+    pass_x = (keep_x + got_y[half:].astype(F32)).astype(BF16)
+    last_y = flip(pass_y, "sp", 2)
+    last_x = flip(pass_x, "sp", 1)
+    near = jnp.concatenate([got_x[:half], got_y[:half]], axis=0).astype(F32)
+    far = jnp.concatenate([last_y, last_x], axis=0).astype(F32)
+    tokens_grad = (own_t + near + far).astype(BF16)
+    (values_grad,) = call(
+        values_kernel,
+        "values",
+        [shape((rows, vcols * sp_count), BF16)],
+        [],
+        "svvvv",
+        1 << 18,
+        8,
+        index, vgrad, *v_out,
+    )
+    (w_sum,) = call(
+        depth_sum_kernel,
+        "depth_sum",
+        [shape((wrows, 2 * cols), BF16)],
+        [],
+        "vvvv",
+        1 << 18,
+        8,
+        own_w, *got_line,
+    )
+    w_x = flip(w_sum, "sp", 1)
+    w_y = flip(w_sum, "sp", 2)
+    w_da = flip(w_x[: wrows // 2], "sp", 2)
+    w_db = flip(w_y[wrows // 2 :], "sp", 1)
+    factor = 1.0 / math.sqrt(dp_count * seq)
+    query_weight_grad, key_weight_grad = call(
+        functools.partial(place_kernel, factor, cols),
+        "place",
+        [shape((wrows, cols * sp_count), F32)] * 2,
+        [],
+        "svvvvv",
+        1 << 18,
+        8,
+        index, w_sum, w_x, w_y, w_da, w_db,
+    )
+    return (tokens_grad[None], values_grad[None], query_weight_grad, key_weight_grad)
+
+
 def solution(mesh):
     in_specs = (
         P("dp", "sp", None),
@@ -197,4 +626,6 @@
         P("dp", "sp", None),
     )
     out_specs = (P("dp", "sp", None), P("dp", "sp", None), P("dp", None), P("dp", None))
+    quarter = mesh.shape["sp"] == 4 and mesh.shape["dp"] == 8
+    body = quarter_body if quarter else general_body
     return jax.shard_map(body, mesh=mesh, in_specs=in_specs, out_specs=out_specs, check_vma=False)

time: 488 us -> 146 us (0.30); the launches traced: 481 us -> 144 us
  waiting for transfers between devices: 200 us -> 63.5 us
  matrix products: 99.6 us -> 0 us
  local copies, waits for them, and re-layouts: 84.4 us -> 6.96 us
  other arithmetic: 53 us -> 3.73 us
  Pallas kernels: 0 us -> 31.5 us
  starting transfers between devices: 17 us -> 37.9 us
  between operations: 14.5 us -> 0.8 us
  blocking collectives: 11.9 us -> 0 us
    reduce_scatter x1 -> x0, waiting for transfers between devices: 79.1 us -> none  [body(): lax.psum_scatter(lax.dot_general(token_block, packed_rows, outer_rows, pr...]
    all_gather x2 -> x0, waiting for transfers between devices: 74.5 us -> none  [the longest x1 43.2 us: body(): lax.all_gather(query_weight, 'dp', axis=0, tiled=True)]
    ppermute x0 -> x29, waiting for transfers between devices: none -> 63.5 us  [flip(): return lax.ppermute(value, axis, [(i, i ^ mask) for i in range(count)])]
    dot_general x25 -> x0, matrix products: 55.3 us -> none  [the longest x20 34.7 us: pair_product(): jnp.einsum(pattern, first_op, second_op, preferred_element_type=jnp.float32)]
    psum x1 -> x0, waiting for transfers between devices: 44.7 us -> none  [body(): grad_total = lax.psum(grad_shard, 'sp').astype(jnp.float32)]
    sub x15 -> x0, matrix products: 44.3 us -> none  [the longest x5 17 us: block_step(): exp_scores = jnp.exp(scores - row_max)]
    ppermute x0 -> x29, starting transfers between devices: none -> 37.9 us  [flip(): return lax.ppermute(value, axis, [(i, i ^ mask) for i in range(count)])]
    pallas_call x0 -> x8, Pallas kernels: none -> 31.5 us  [call(): pl.pallas_call(kernel, name=name, out_shape=outs, in_specs=[smem if k ==...]
  transfers between devices with their start and end apart: 8 -> 29, of which waited for: 5 -> 13; matrix products, arithmetic and copies ran while one was open for 16% -> 4% of each run, Pallas kernels for 0% -> 4%
where the time goes in v1:
time: 146 us; the launch traced here: 144 us
  waiting for transfers between devices  63.5 us (43%)
  starting transfers between devices  37.9 us (26%)
  Pallas kernels  31.5 us (22%)
  local copies, waits for them, and re-layouts  6.96 us (5%)
  other arithmetic  3.73 us (3%)
    ppermute x29, waiting for transfers between devices, flip(): return lax.ppermute(value, axis, [(i, i ^ mask) for i in range(count)])  63.5 us
    ppermute x29, starting transfers between devices, flip(): return lax.ppermute(value, axis, [(i, i ^ mask) for i in range(count)])  37.9 us
    pallas_call x8, Pallas kernels, call(): pl.pallas_call(kernel, name=name, out_shape=outs, in_specs=[smem if k ==...  31.5 us
    unnamed x22, local copies, waits for them, and re-layouts  4.89 us
  transfers between devices with their start and end apart: 29, of which 13 were waited for; matrix products, arithmetic and copies ran while one was open for 4% of the time, Pallas kernels for 4%

profile of v1, /device:TPU:0, one launch (start us, length us, event | category | flops | bytes accessed | tf_op | source)
XLA Modules:
  0.0 144.4 jit_solution(8750709437594320697)
XLA Ops:
  0.6 3.0 %collective-permute-start = (bf16[160,2048]{1,0:T(8,128)(2,1)}, bf16[160,2048]{1,0:T(8,128)(2,1)S(1)}, u32[]{:S(2)}, u32[]{:S(2)}) collective-permute-start(bf16[160,2048]{1,0:T(8,128)(2,1)} %bitcast.11), channel_id=1, source_target_pairs={{0,8},{8,0},{16,24},{24,16},{1,9},{9,1},{17,25},{25,17},{2,10},{10... | collective-permute-start | bytes 1966088 | tf_op jit(solution)/shard_map/ppermute | solution.py:468
  3.7 1.5 %collective-permute-start.1 = (bf16[160,2048]{1,0:T(8,128)(2,1)}, bf16[160,2048]{1,0:T(8,128)(2,1)S(1)}, u32[]{:S(2)}, u32[]{:S(2)}) collective-permute-start(bf16[160,2048]{1,0:T(8,128)(2,1)} %bitcast.12), channel_id=1, source_target_pairs={{0,16},{8,24},{16,0},{24,8},{1,17},{9,25},{17,1},{25,9},{2,18},{10... | collective-permute-start | bytes 1966088 | tf_op jit(solution)/shard_map/ppermute | solution.py:468
  10.6 4.1 %collective-permute-start.6 = (bf16[256,512]{1,0:T(8,128)(2,1)S(1)}, bf16[256,512]{1,0:T(8,128)(2,1)S(1)}, u32[]{:S(2)}, u32[]{:S(2)}) collective-permute-start(bf16[256,512]{1,0:T(8,128)(2,1)S(1)} %get-tuple-element.27.w0), channel_id=1, source_target_pairs={{0,6},{1,7},{2,4},{3,5},{4,2},{5,3},{6,0},{7,1},{8,14},{9,15},{10,... | collective-permute-start | bytes 786440 | tf_op jit(solution)/shard_map/ppermute | solution.py:468
  14.7 7.4 %collective-permute-done.11.g1 = bf16[160,512]{1,0:T(8,128)(2,1)S(1)} collective-permute-done((bf16[160,512]{1,0:T(8,128)(2,1)S(1)}, bf16[160,512]{1,0:T(8,128)(2,1)S(1)}, u32[]{:S(2)}, u32[]{:S(2)}) %collective-permute-start.11) | collective-permute-done | bytes 163872 | tf_op jit(solution)/shard_map/ppermute | solution.py:468
  22.1 1.8 %collective-permute-start.4 = (bf16[256,512]{1,0:T(8,128)(2,1)S(1)}, bf16[256,512]{1,0:T(8,128)(2,1)S(1)}, u32[]{:S(2)}, u32[]{:S(2)}) collective-permute-start(bf16[256,512]{1,0:T(8,128)(2,1)S(1)} %get-tuple-element.27.w0), channel_id=1, source_target_pairs={{0,2},{1,3},{2,0},{3,1},{4,6},{5,7},{6,4},{7,5},{8,10},{9,11},{10,... | collective-permute-start | bytes 786440 | tf_op jit(solution)/shard_map/ppermute | solution.py:468
  23.9 2.6 %collective-permute-start.5 = (bf16[256,512]{1,0:T(8,128)(2,1)S(1)}, bf16[256,512]{1,0:T(8,128)(2,1)S(1)}, u32[]{:S(2)}, u32[]{:S(2)}) collective-permute-start(bf16[256,512]{1,0:T(8,128)(2,1)S(1)} %get-tuple-element.27.w0), channel_id=1, source_target_pairs={{0,4},{1,5},{2,6},{3,7},{4,0},{5,1},{6,2},{7,3},{8,12},{9,13},{10,... | collective-permute-start | bytes 786440 | tf_op jit(solution)/shard_map/ppermute | solution.py:468
  26.5 2.5 %collective-permute-start.13 = (bf16[160,512]{1,0:T(8,128)(2,1)S(1)}, bf16[160,512]{1,0:T(8,128)(2,1)S(1)}, u32[]{:S(2)}, u32[]{:S(2)}) collective-permute-start(bf16[160,512]{1,0:T(8,128)(2,1)S(1)} %get-tuple-element.31), channel_id=1, source_target_pairs={{0,24},{8,16},{16,8},{24,0},{1,25},{9,17},{17,9},{25,1},{2,26},{10... | collective-permute-start | bytes 491528 | tf_op jit(solution)/shard_map/ppermute | solution.py:468
  29.4 5.7 %collective-permute-done.4.w1 = bf16[256,512]{1,0:T(8,128)(2,1)S(1)} collective-permute-done((bf16[256,512]{1,0:T(8,128)(2,1)S(1)}, bf16[256,512]{1,0:T(8,128)(2,1)S(1)}, u32[]{:S(2)}, u32[]{:S(2)}) %collective-permute-start.4) | collective-permute-done | bytes 262176 | tf_op jit(solution)/shard_map/ppermute | solution.py:468
  35.1 2.3 %collective-permute-done.5.w2 = bf16[256,512]{1,0:T(8,128)(2,1)S(1)} collective-permute-done((bf16[256,512]{1,0:T(8,128)(2,1)S(1)}, bf16[256,512]{1,0:T(8,128)(2,1)S(1)}, u32[]{:S(2)}, u32[]{:S(2)}) %collective-permute-start.5) | collective-permute-done | bytes 262176 | tf_op jit(solution)/shard_map/ppermute | solution.py:468
  37.4 1.5 %collective-permute-start.2 = (bf16[80,2048]{1,0:T(8,128)(2,1)S(1)}, bf16[80,2048]{1,0:T(8,128)(2,1)S(1)}, u32[]{:S(2)}, u32[]{:S(2)}) collective-permute-start(bf16[80,2048]{1,0:T(8,128)(2,1)S(1)} %slice.32), channel_id=1, source_target_pairs={{0,16},{8,24},{16,0},{24,8},{1,17},{9,25},{17,1},{25,9},{2,18},{10... | collective-permute-start | bytes 983048 | tf_op jit(solution)/shard_map/ppermute | solution.py:468
  38.9 1.5 %collective-permute-start.3 = (bf16[80,2048]{1,0:T(8,128)(2,1)S(1)}, bf16[80,2048]{1,0:T(8,128)(2,1)S(1)}, u32[]{:S(2)}, u32[]{:S(2)}) collective-permute-start(bf16[80,2048]{1,0:T(8,128)(2,1)S(1)} %slice.33), channel_id=1, source_target_pairs={{0,8},{8,0},{16,24},{24,16},{1,9},{9,1},{17,25},{25,17},{2,10},{10... | collective-permute-start | bytes 983048 | tf_op jit(solution)/shard_map/ppermute | solution.py:468
  40.7 6.8 %collective-permute-done.2.t_da = bf16[80,2048]{1,0:T(8,128)(2,1)S(1)} collective-permute-done((bf16[80,2048]{1,0:T(8,128)(2,1)S(1)}, bf16[80,2048]{1,0:T(8,128)(2,1)S(1)}, u32[]{:S(2)}, u32[]{:S(2)}) %collective-permute-start.2) | collective-permute-done | bytes 327712 | tf_op jit(solution)/shard_map/ppermute | solution.py:468
  48.8 20.2 %attention.1 = (bf16[640,2048]{1,0:T(8,128)(2,1)S(1)}, bf16[2048,512]{1,0:T(8,128)(2,1)S(1)}, bf16[512,640]{1,0:T(8,128)(2,1)S(1)}, bf16[640,512]{1,0:T(8,128)(2,1)S(1)}, bf16[640,256]{1,0:T(8,128)(2,1)S(1)}) custom-call(s32[3]{0:T(128)S(1)} %pad_add_fusion.index, f32[16]{0:T(128)S(1)} %copy-done.10, f32[16,640]{1,0:T(8,128)S(1)} %get-tuple-element.54.cosine, ...), custom_call_target="tpu_custom_call" | custom-call | flops 3355443200 | bytes 11812940 | tf_op jit(solution)/shard_map/attention/pallas_call | solution.py:207
  69.0 3.0 %token_grad.1 = (bf16[160,2048]{1,0:T(8,128)(2,1)}, bf16[160,2048]{1,0:T(8,128)(2,1)}, f32[80,2048]{1,0:T(8,128)S(1)}, f32[80,2048]{1,0:T(8,128)S(1)}, f32[160,2048]{1,0:T(8,128)S(1)}) custom-call(s32[3]{0:T(128)S(1)} %pad_add_fusion.index, bf16[640,512]{1,0:T(8,128)(2,1)S(1)} %get-tuple-element.32.back, bf16[2048,512]{1,0:T(8,128)(2,1)S(1)} %get-tuple-element.33.wfull), custom_call_target="tpu_custom_call" | custom-call | flops 1342177280 | bytes 6684684 | tf_op jit(solution)/shard_map/token_grad/pallas_call | solution.py:207
  72.9 1.5 %collective-permute-start.14 = (bf16[160,2048]{1,0:T(8,128)(2,1)}, bf16[160,2048]{1,0:T(8,128)(2,1)}, u32[]{:S(2)}, u32[]{:S(2)}) collective-permute-start(bf16[160,2048]{1,0:T(8,128)(2,1)} %get-tuple-element.35), channel_id=1, source_target_pairs={{0,8},{8,0},{16,24},{24,16},{1,9},{9,1},{17,25},{25,17},{2,10},{10... | collective-permute-start | bytes 1966088 | tf_op jit(solution)/shard_map/ppermute | solution.py:468
  74.4 3.3 %weight_grad.1 = (bf16[4,512,256]{2,1,0:T(8,128)(2,1)S(1)}, bf16[4,512,256]{2,1,0:T(8,128)(2,1)}) custom-call(s32[3]{0:T(128)S(1)} %pad_add_fusion.index, bf16[512,640]{1,0:T(8,128)(2,1)S(1)} %get-tuple-element.40.back_t, bf16[640,2048]{1,0:T(8,128)(2,1)S(1)} %get-tuple-element.41.tok), custom_call_target="tpu_custom_call" | custom-call | flops 1342177280 | bytes 5373964 | tf_op jit(solution)/shard_map/weight_grad/pallas_call | solution.py:207
  78.2 11.0 %collective-permute-done.14 = bf16[160,2048]{1,0:T(8,128)(2,1)} collective-permute-done((bf16[160,2048]{1,0:T(8,128)(2,1)}, bf16[160,2048]{1,0:T(8,128)(2,1)}, u32[]{:S(2)}, u32[]{:S(2)}) %collective-permute-start.14) | collective-permute-done | bytes 655392 | tf_op jit(solution)/shard_map/ppermute | solution.py:468
  92.4 3.3 %collective-permute-start.23 = (bf16[512,256]{1,0:T(8,128)(2,1)S(1)}, bf16[512,256]{1,0:T(8,128)(2,1)S(1)}, u32[]{:S(2)}, u32[]{:S(2)}) collective-permute-start(bf16[512,256]{1,0:T(8,128)(2,1)S(1)} %get-tuple-element.46), channel_id=1, source_target_pairs={{0,4},{1,5},{2,6},{3,7},{4,0},{5,1},{6,2},{7,3},{8,12},{9,13},{10,... | collective-permute-start | bytes 786440 | tf_op jit(solution)/shard_map/ppermute | solution.py:468
  97.4 1.6 %collective-permute-start.17 = (bf16[80,2048]{1,0:T(8,128)(2,1)S(1)}, bf16[80,2048]{1,0:T(8,128)(2,1)S(1)}, u32[]{:S(2)}, u32[]{:S(2)}) collective-permute-start(bf16[80,2048]{1,0:T(8,128)(2,1)S(1)} %add_convert_fusion.1), channel_id=1, source_target_pairs={{0,8},{8,0},{16,24},{24,16},{1,9},{9,1},{17,25},{25,17},{2,10},{10... | collective-permute-start | bytes 983048 | tf_op jit(solution)/shard_map/ppermute | solution.py:468
  99.0 3.6 %collective-permute-done.22.r1 = bf16[512,256]{1,0:T(8,128)(2,1)S(1)} collective-permute-done((bf16[512,256]{1,0:T(8,128)(2,1)S(1)}, bf16[512,256]{1,0:T(8,128)(2,1)S(1)}, u32[]{:S(2)}, u32[]{:S(2)}) %collective-permute-start.22) | collective-permute-done | bytes 262176 | tf_op jit(solution)/shard_map/ppermute | solution.py:468
  102.6 11.5 %collective-permute-done.23.r2 = bf16[512,256]{1,0:T(8,128)(2,1)S(1)} collective-permute-done((bf16[512,256]{1,0:T(8,128)(2,1)S(1)}, bf16[512,256]{1,0:T(8,128)(2,1)S(1)}, u32[]{:S(2)}, u32[]{:S(2)}) %collective-permute-start.23) | collective-permute-done | bytes 262176 | tf_op jit(solution)/shard_map/ppermute | solution.py:468
  115.4 1.4 collective-permute-start.26
  117.9 3.7 %collective-permute-done.18.r1 = bf16[160,256]{1,0:T(8,128)(2,1)S(1)} collective-permute-done((bf16[160,256]{1,0:T(8,128)(2,1)S(1)}, bf16[160,256]{1,0:T(8,128)(2,1)S(1)}, u32[]{:S(2)}, u32[]{:S(2)}) %collective-permute-start.18) | collective-permute-done | bytes 81952 | tf_op jit(solution)/shard_map/ppermute | solution.py:468
  121.6 1.6 %collective-permute-start.19 = (bf16[160,256]{1,0:T(8,128)(2,1)S(1)}, bf16[160,256]{1,0:T(8,128)(2,1)S(1)}, u32[]{:S(2)}, u32[]{:S(2)}) collective-permute-start(bf16[160,256]{1,0:T(8,128)(2,1)S(1)} %get-tuple-element.51), channel_id=1, source_target_pairs={{0,16},{8,24},{16,0},{24,8},{1,17},{9,25},{17,1},{25,9},{2,18},{10... | collective-permute-start | bytes 245768 | tf_op jit(solution)/shard_map/ppermute | solution.py:468
  123.2 2.8 %collective-permute-done.19.r2 = bf16[160,256]{1,0:T(8,128)(2,1)S(1)} collective-permute-done((bf16[160,256]{1,0:T(8,128)(2,1)S(1)}, bf16[160,256]{1,0:T(8,128)(2,1)S(1)}, u32[]{:S(2)}, u32[]{:S(2)}) %collective-permute-start.19) | collective-permute-done | bytes 81952 | tf_op jit(solution)/shard_map/ppermute | solution.py:468
  126.1 2.1 %collective-permute-start.20 = (bf16[160,256]{1,0:T(8,128)(2,1)S(1)}, bf16[160,256]{1,0:T(8,128)(2,1)S(1)}, u32[]{:S(2)}, u32[]{:S(2)}) collective-permute-start(bf16[160,256]{1,0:T(8,128)(2,1)S(1)} %get-tuple-element.50), channel_id=1, source_target_pairs={{0,24},{8,16},{16,8},{24,0},{1,25},{9,17},{17,9},{25,1},{2,26},{10... | collective-permute-start | bytes 245768 | tf_op jit(solution)/shard_map/ppermute | solution.py:468
  128.2 4.1 %collective-permute-done.20.r3 = bf16[160,256]{1,0:T(8,128)(2,1)S(1)} collective-permute-done((bf16[160,256]{1,0:T(8,128)(2,1)S(1)}, bf16[160,256]{1,0:T(8,128)(2,1)S(1)}, u32[]{:S(2)}, u32[]{:S(2)}) %collective-permute-start.20) | collective-permute-done | bytes 81952 | tf_op jit(solution)/shard_map/ppermute | solution.py:468
  132.3 1.3 values.1
  135.6 1.7 %collective-permute-start.27 = (bf16[128,512]{1,0:T(8,128)(2,1)S(1)}, bf16[128,512]{1,0:T(8,128)(2,1)S(1)}, u32[]{:S(2)}, u32[]{:S(2)}) collective-permute-start(bf16[128,512]{1,0:T(8,128)(2,1)S(1)} %slice.38), channel_id=1, source_target_pairs={{0,16},{8,24},{16,0},{24,8},{1,17},{9,25},{17,1},{25,9},{2,18},{10... | collective-permute-start | bytes 393224 | tf_op jit(solution)/shard_map/ppermute | solution.py:468
  139.2 1.4 collective-permute-done.27.da
  140.6 1.7 %collective-permute-done.28.db = bf16[128,512]{1,0:T(8,128)(2,1)S(1)} collective-permute-done((bf16[128,512]{1,0:T(8,128)(2,1)S(1)}, bf16[128,512]{1,0:T(8,128)(2,1)S(1)}, u32[]{:S(2)}, u32[]{:S(2)}) %collective-permute-start.28) | collective-permute-done | bytes 131104 | tf_op jit(solution)/shard_map/ppermute | solution.py:468
  142.3 2.0 %place.1 = (f32[256,1024]{1,0:T(8,128)}, f32[256,1024]{1,0:T(8,128)}) custom-call(s32[3]{0:T(128)S(1)} %pad_add_fusion.index, bf16[256,512]{1,0:T(8,128)(2,1)S(1)} %depth_sum.1.own, bf16[256,512]{1,0:T(8,128)(2,1)S(1)} %collective-permute-done.25.got_x, bf16[256,512]{1,0:T(8,128)(2,1)S(1)} %collective-permute-done.26.got_y, ...), custom_call_target="tpu_custom_call" | custom-call | flops 262144 | bytes 3145740 | tf_op jit(solution)/shard_map/place/pallas_call | solution.py:207
  (70 shorter events, 19.8 us)
Async XLA Ops:
  0.6 25.9 %collective-permute-start = (bf16[160,2048]{1,0:T(8,128)(2,1)}, bf16[160,2048]{1,0:T(8,128)(2,1)S(1)}, u32[]{:S(2)}, u32[]{:S(2)}) collective-permute-start(bf16[160,2048]{1,0:T(8,128)(2,1)} %bitcast.11), channel_id=1, source_target_pairs={{0,8},{8,0},{16,24},{24,16},{1,9},{9,1},{17,25},{25,17},{2,10},{10... | collective-permute-start | bytes 1966088 | tf_op jit(solution)/shard_map/ppermute | solution.py:468
  3.7 22.9 %collective-permute-start.1 = (bf16[160,2048]{1,0:T(8,128)(2,1)}, bf16[160,2048]{1,0:T(8,128)(2,1)S(1)}, u32[]{:S(2)}, u32[]{:S(2)}) collective-permute-start(bf16[160,2048]{1,0:T(8,128)(2,1)} %bitcast.12), channel_id=1, source_target_pairs={{0,16},{8,24},{16,0},{24,8},{1,17},{9,25},{17,1},{25,9},{2,18},{10... | collective-permute-start | bytes 1966088 | tf_op jit(solution)/shard_map/ppermute | solution.py:468
  9.3 39.5 %copy-start.9 = (bf16[1,160,2048]{2,1,0:T(8,128)(2,1)S(1)}, bf16[1,160,2048]{2,1,0:T(8,128)(2,1)}, u32[]{:S(2)}) copy-start(bf16[1,160,2048]{2,1,0:T(8,128)(2,1)} %param.6) | copy-start | bytes 1966084
  9.3 39.5 %copy-start.10 = (f32[16]{0:T(128)S(1)}, f32[16]{0:T(128)}, u32[]{:S(2)}) copy-start(f32[16]{0:T(128)} %lambdas.1) | copy-start | bytes 196
  10.0 12.2 %collective-permute-start.11 = (bf16[160,512]{1,0:T(8,128)(2,1)S(1)}, bf16[160,512]{1,0:T(8,128)(2,1)S(1)}, u32[]{:S(2)}, u32[]{:S(2)}) collective-permute-start(bf16[160,512]{1,0:T(8,128)(2,1)S(1)} %get-tuple-element.29), channel_id=1, source_target_pairs={{0,8},{8,0},{16,24},{24,16},{1,9},{9,1},{17,25},{25,17},{2,10},{10... | collective-permute-start | bytes 491528 | tf_op jit(solution)/shard_map/ppermute | solution.py:468
  10.6 13.4 %collective-permute-start.12 = (bf16[160,512]{1,0:T(8,128)(2,1)S(1)}, bf16[160,512]{1,0:T(8,128)(2,1)S(1)}, u32[]{:S(2)}, u32[]{:S(2)}) collective-permute-start(bf16[160,512]{1,0:T(8,128)(2,1)S(1)} %get-tuple-element.30), channel_id=1, source_target_pairs={{0,16},{8,24},{16,0},{24,8},{1,17},{9,25},{17,1},{25,9},{2,18},{10... | collective-permute-start | bytes 491528 | tf_op jit(solution)/shard_map/ppermute | solution.py:468
  10.6 18.5 %collective-permute-start.6 = (bf16[256,512]{1,0:T(8,128)(2,1)S(1)}, bf16[256,512]{1,0:T(8,128)(2,1)S(1)}, u32[]{:S(2)}, u32[]{:S(2)}) collective-permute-start(bf16[256,512]{1,0:T(8,128)(2,1)S(1)} %get-tuple-element.27.w0), channel_id=1, source_target_pairs={{0,6},{1,7},{2,4},{3,5},{4,2},{5,3},{6,0},{7,1},{8,14},{9,15},{10,... | collective-permute-start | bytes 786440 | tf_op jit(solution)/shard_map/ppermute | solution.py:468
  22.1 13.0 %collective-permute-start.4 = (bf16[256,512]{1,0:T(8,128)(2,1)S(1)}, bf16[256,512]{1,0:T(8,128)(2,1)S(1)}, u32[]{:S(2)}, u32[]{:S(2)}) collective-permute-start(bf16[256,512]{1,0:T(8,128)(2,1)S(1)} %get-tuple-element.27.w0), channel_id=1, source_target_pairs={{0,2},{1,3},{2,0},{3,1},{4,6},{5,7},{6,4},{7,5},{8,10},{9,11},{10,... | collective-permute-start | bytes 786440 | tf_op jit(solution)/shard_map/ppermute | solution.py:468
  23.9 13.5 %collective-permute-start.5 = (bf16[256,512]{1,0:T(8,128)(2,1)S(1)}, bf16[256,512]{1,0:T(8,128)(2,1)S(1)}, u32[]{:S(2)}, u32[]{:S(2)}) collective-permute-start(bf16[256,512]{1,0:T(8,128)(2,1)S(1)} %get-tuple-element.27.w0), channel_id=1, source_target_pairs={{0,4},{1,5},{2,6},{3,7},{4,0},{5,1},{6,2},{7,3},{8,12},{9,13},{10,... | collective-permute-start | bytes 786440 | tf_op jit(solution)/shard_map/ppermute | solution.py:468
  26.5 12.4 %collective-permute-start.7 = (bf16[256,512]{1,0:T(8,128)(2,1)S(1)}, bf16[256,512]{1,0:T(8,128)(2,1)S(1)}, u32[]{:S(2)}, u32[]{:S(2)}) collective-permute-start(bf16[256,512]{1,0:T(8,128)(2,1)S(1)} %get-tuple-element.27.w0), channel_id=1, source_target_pairs={{0,1},{1,0},{2,3},{3,2},{4,5},{5,4},{6,7},{7,6},{8,9},{9,8},{10,11... | collective-permute-start | bytes 786440 | tf_op jit(solution)/shard_map/ppermute | solution.py:468
  26.5 10.9 %collective-permute-start.13 = (bf16[160,512]{1,0:T(8,128)(2,1)S(1)}, bf16[160,512]{1,0:T(8,128)(2,1)S(1)}, u32[]{:S(2)}, u32[]{:S(2)}) collective-permute-start(bf16[160,512]{1,0:T(8,128)(2,1)S(1)} %get-tuple-element.31), channel_id=1, source_target_pairs={{0,24},{8,16},{16,8},{24,0},{1,25},{9,17},{17,9},{25,1},{2,26},{10... | collective-permute-start | bytes 491528 | tf_op jit(solution)/shard_map/ppermute | solution.py:468
  29.1 11.6 %collective-permute-start.10 = (bf16[256,512]{1,0:T(8,128)(2,1)S(1)}, bf16[256,512]{1,0:T(8,128)(2,1)S(1)}, u32[]{:S(2)}, u32[]{:S(2)}) collective-permute-start(bf16[256,512]{1,0:T(8,128)(2,1)S(1)} %collective-permute-done.6.w3), channel_id=1, source_target_pairs={{0,1},{1,0},{2,3},{3,2},{4,5},{5,4},{6,7},{7,6},{8,9},{9,8},{10,11... | collective-permute-start | bytes 786440 | tf_op jit(solution)/shard_map/ppermute | solution.py:468
  35.1 5.6 %collective-permute-start.8 = (bf16[256,512]{1,0:T(8,128)(2,1)S(1)}, bf16[256,512]{1,0:T(8,128)(2,1)S(1)}, u32[]{:S(2)}, u32[]{:S(2)}) collective-permute-start(bf16[256,512]{1,0:T(8,128)(2,1)S(1)} %collective-permute-done.4.w1), channel_id=1, source_target_pairs={{0,1},{1,0},{2,3},{3,2},{4,5},{5,4},{6,7},{7,6},{8,9},{9,8},{10,11... | collective-permute-start | bytes 786440 | tf_op jit(solution)/shard_map/ppermute | solution.py:468
  37.4 3.3 %collective-permute-start.9 = (bf16[256,512]{1,0:T(8,128)(2,1)S(1)}, bf16[256,512]{1,0:T(8,128)(2,1)S(1)}, u32[]{:S(2)}, u32[]{:S(2)}) collective-permute-start(bf16[256,512]{1,0:T(8,128)(2,1)S(1)} %collective-permute-done.5.w2), channel_id=1, source_target_pairs={{0,1},{1,0},{2,3},{3,2},{4,5},{5,4},{6,7},{7,6},{8,9},{9,8},{10,11... | collective-permute-start | bytes 786440 | tf_op jit(solution)/shard_map/ppermute | solution.py:468
  37.4 10.1 %collective-permute-start.2 = (bf16[80,2048]{1,0:T(8,128)(2,1)S(1)}, bf16[80,2048]{1,0:T(8,128)(2,1)S(1)}, u32[]{:S(2)}, u32[]{:S(2)}) collective-permute-start(bf16[80,2048]{1,0:T(8,128)(2,1)S(1)} %slice.32), channel_id=1, source_target_pairs={{0,16},{8,24},{16,0},{24,8},{1,17},{9,25},{17,1},{25,9},{2,18},{10... | collective-permute-start | bytes 983048 | tf_op jit(solution)/shard_map/ppermute | solution.py:468
  38.9 9.8 %collective-permute-start.3 = (bf16[80,2048]{1,0:T(8,128)(2,1)S(1)}, bf16[80,2048]{1,0:T(8,128)(2,1)S(1)}, u32[]{:S(2)}, u32[]{:S(2)}) collective-permute-start(bf16[80,2048]{1,0:T(8,128)(2,1)S(1)} %slice.33), channel_id=1, source_target_pairs={{0,8},{8,0},{16,24},{24,16},{1,9},{9,1},{17,25},{25,17},{2,10},{10... | collective-permute-start | bytes 983048 | tf_op jit(solution)/shard_map/ppermute | solution.py:468
  72.9 16.3 %collective-permute-start.14 = (bf16[160,2048]{1,0:T(8,128)(2,1)}, bf16[160,2048]{1,0:T(8,128)(2,1)}, u32[]{:S(2)}, u32[]{:S(2)}) collective-permute-start(bf16[160,2048]{1,0:T(8,128)(2,1)} %get-tuple-element.35), channel_id=1, source_target_pairs={{0,8},{8,0},{16,24},{24,16},{1,9},{9,1},{17,25},{25,17},{2,10},{10... | collective-permute-start | bytes 1966088 | tf_op jit(solution)/shard_map/ppermute | solution.py:468
  77.7 13.4 %collective-permute-start.21 = (bf16[4,512,256]{2,1,0:T(8,128)(2,1)}, bf16[4,512,256]{2,1,0:T(8,128)(2,1)S(1)}, u32[]{:S(2)}, u32[]{:S(2)}) collective-permute-start(bf16[4,512,256]{2,1,0:T(8,128)(2,1)} %get-tuple-element.43), channel_id=1, source_target_pairs={{0,1},{1,0},{2,3},{3,2},{4,5},{5,4},{6,7},{7,6},{8,9},{9,8},{10,11... | collective-permute-start | bytes 3145736 | tf_op jit(solution)/shard_map/ppermute | solution.py:468
  77.7 18.6 %collective-permute-start.15 = (bf16[160,2048]{1,0:T(8,128)(2,1)}, bf16[160,2048]{1,0:T(8,128)(2,1)}, u32[]{:S(2)}, u32[]{:S(2)}) collective-permute-start(bf16[160,2048]{1,0:T(8,128)(2,1)} %get-tuple-element.36), channel_id=1, source_target_pairs={{0,16},{8,24},{16,0},{24,8},{1,17},{9,25},{17,1},{25,9},{2,18},{10... | collective-permute-start | bytes 1966088 | tf_op jit(solution)/shard_map/ppermute | solution.py:468
  90.4 47.7 %collective-permute-start.16 = (bf16[80,2048]{1,0:T(8,128)(2,1)S(1)}, bf16[80,2048]{1,0:T(8,128)(2,1)S(1)}, u32[]{:S(2)}, u32[]{:S(2)}) collective-permute-start(bf16[80,2048]{1,0:T(8,128)(2,1)S(1)} %add_convert_fusion.2), channel_id=1, source_target_pairs={{0,16},{8,24},{16,0},{24,8},{1,17},{9,25},{17,1},{25,9},{2,18},{10... | collective-permute-start | bytes 983048 | tf_op jit(solution)/shard_map/ppermute | solution.py:468
  91.9 10.8 %collective-permute-start.22 = (bf16[512,256]{1,0:T(8,128)(2,1)S(1)}, bf16[512,256]{1,0:T(8,128)(2,1)S(1)}, u32[]{:S(2)}, u32[]{:S(2)}) collective-permute-start(bf16[512,256]{1,0:T(8,128)(2,1)S(1)} %get-tuple-element.45), channel_id=1, source_target_pairs={{0,2},{1,3},{2,0},{3,1},{4,6},{5,7},{6,4},{7,5},{8,10},{9,11},{10,... | collective-permute-start | bytes 786440 | tf_op jit(solution)/shard_map/ppermute | solution.py:468
  92.4 21.7 %collective-permute-start.23 = (bf16[512,256]{1,0:T(8,128)(2,1)S(1)}, bf16[512,256]{1,0:T(8,128)(2,1)S(1)}, u32[]{:S(2)}, u32[]{:S(2)}) collective-permute-start(bf16[512,256]{1,0:T(8,128)(2,1)S(1)} %get-tuple-element.46), channel_id=1, source_target_pairs={{0,4},{1,5},{2,6},{3,7},{4,0},{5,1},{6,2},{7,3},{8,12},{9,13},{10,... | collective-permute-start | bytes 786440 | tf_op jit(solution)/shard_map/ppermute | solution.py:468
  95.7 18.4 %collective-permute-start.24 = (bf16[512,256]{1,0:T(8,128)(2,1)S(1)}, bf16[512,256]{1,0:T(8,128)(2,1)S(1)}, u32[]{:S(2)}, u32[]{:S(2)}) collective-permute-start(bf16[512,256]{1,0:T(8,128)(2,1)S(1)} %get-tuple-element.47), channel_id=1, source_target_pairs={{0,6},{1,7},{2,4},{3,5},{4,2},{5,3},{6,0},{7,1},{8,14},{9,15},{10,... | collective-permute-start | bytes 786440 | tf_op jit(solution)/shard_map/ppermute | solution.py:468
  96.3 20.4 %copy-start.1 = (bf16[640,256]{1,0:T(8,128)(2,1)S(1)}, bf16[640,256]{1,0:T(8,128)(2,1)}, u32[]{:S(2)}) copy-start(bf16[640,256]{1,0:T(8,128)(2,1)} %copy-done) | copy-start | bytes 983044
  97.4 40.7 %collective-permute-start.17 = (bf16[80,2048]{1,0:T(8,128)(2,1)S(1)}, bf16[80,2048]{1,0:T(8,128)(2,1)S(1)}, u32[]{:S(2)}, u32[]{:S(2)}) collective-permute-start(bf16[80,2048]{1,0:T(8,128)(2,1)S(1)} %add_convert_fusion.1), channel_id=1, source_target_pairs={{0,8},{8,0},{16,24},{24,16},{1,9},{9,1},{17,25},{25,17},{2,10},{10... | collective-permute-start | bytes 983048 | tf_op jit(solution)/shard_map/ppermute | solution.py:468
  114.3 21.3 %collective-permute-start.25 = (bf16[256,512]{1,0:T(8,128)(2,1)S(1)}, bf16[256,512]{1,0:T(8,128)(2,1)S(1)}, u32[]{:S(2)}, u32[]{:S(2)}) collective-permute-start(bf16[256,512]{1,0:T(8,128)(2,1)S(1)} %depth_sum.1.own), channel_id=1, source_target_pairs={{0,8},{8,0},{16,24},{24,16},{1,9},{9,1},{17,25},{25,17},{2,10},{10... | collective-permute-start | bytes 786440 | tf_op jit(solution)/shard_map/ppermute | solution.py:468
  115.4 21.9 %collective-permute-start.26 = (bf16[256,512]{1,0:T(8,128)(2,1)S(1)}, bf16[256,512]{1,0:T(8,128)(2,1)S(1)}, u32[]{:S(2)}, u32[]{:S(2)}) collective-permute-start(bf16[256,512]{1,0:T(8,128)(2,1)S(1)} %depth_sum.1.own), channel_id=1, source_target_pairs={{0,16},{8,24},{16,0},{24,8},{1,17},{9,25},{17,1},{25,9},{2,18},{10... | collective-permute-start | bytes 786440 | tf_op jit(solution)/shard_map/ppermute | solution.py:468
  116.8 4.9 %collective-permute-start.18 = (bf16[160,256]{1,0:T(8,128)(2,1)S(1)}, bf16[160,256]{1,0:T(8,128)(2,1)S(1)}, u32[]{:S(2)}, u32[]{:S(2)}) collective-permute-start(bf16[160,256]{1,0:T(8,128)(2,1)S(1)} %get-tuple-element.52), channel_id=1, source_target_pairs={{0,8},{8,0},{16,24},{24,16},{1,9},{9,1},{17,25},{25,17},{2,10},{10... | collective-permute-start | bytes 245768 | tf_op jit(solution)/shard_map/ppermute | solution.py:468
  121.6 4.4 %collective-permute-start.19 = (bf16[160,256]{1,0:T(8,128)(2,1)S(1)}, bf16[160,256]{1,0:T(8,128)(2,1)S(1)}, u32[]{:S(2)}, u32[]{:S(2)}) collective-permute-start(bf16[160,256]{1,0:T(8,128)(2,1)S(1)} %get-tuple-element.51), channel_id=1, source_target_pairs={{0,16},{8,24},{16,0},{24,8},{1,17},{9,25},{17,1},{25,9},{2,18},{10... | collective-permute-start | bytes 245768 | tf_op jit(solution)/shard_map/ppermute | solution.py:468
  126.1 6.2 %collective-permute-start.20 = (bf16[160,256]{1,0:T(8,128)(2,1)S(1)}, bf16[160,256]{1,0:T(8,128)(2,1)S(1)}, u32[]{:S(2)}, u32[]{:S(2)}) collective-permute-start(bf16[160,256]{1,0:T(8,128)(2,1)S(1)} %get-tuple-element.50), channel_id=1, source_target_pairs={{0,24},{8,16},{16,8},{24,0},{1,25},{9,17},{17,9},{25,1},{2,26},{10... | collective-permute-start | bytes 245768 | tf_op jit(solution)/shard_map/ppermute | solution.py:468
  135.6 5.0 %collective-permute-start.27 = (bf16[128,512]{1,0:T(8,128)(2,1)S(1)}, bf16[128,512]{1,0:T(8,128)(2,1)S(1)}, u32[]{:S(2)}, u32[]{:S(2)}) collective-permute-start(bf16[128,512]{1,0:T(8,128)(2,1)S(1)} %slice.38), channel_id=1, source_target_pairs={{0,16},{8,24},{16,0},{24,8},{1,17},{9,25},{17,1},{25,9},{2,18},{10... | collective-permute-start | bytes 393224 | tf_op jit(solution)/shard_map/ppermute | solution.py:468
  137.3 5.0 %collective-permute-start.28 = (bf16[128,512]{1,0:T(8,128)(2,1)S(1)}, bf16[128,512]{1,0:T(8,128)(2,1)S(1)}, u32[]{:S(2)}, u32[]{:S(2)}) collective-permute-start(bf16[128,512]{1,0:T(8,128)(2,1)S(1)} %slice.39), channel_id=1, source_target_pairs={{0,8},{8,0},{16,24},{24,16},{1,9},{9,1},{17,25},{25,17},{2,10},{10... | collective-permute-start | bytes 393224 | tf_op jit(solution)/shard_map/ppermute | solution.py:468
  (8 other events, 18.6 us)
